TPU v7x, 32 devices: a whole 2x2x4 slice. The times are simulated.
32 devices in a mesh: kv: 4 (over y, x), tp: 8 (over z, core).
Axes of the slice: x: 2, y: 2, z: 4, core: 2. Of those that a mesh axis runs over, the one named last changes fastest.
Arguments:
- residual: bfloat16 [128, 4096], P(None, ('kv', 'tp')), may hold values from -20 to 20
- mixer_gain: float32 [4096], P('kv'), may hold values from 0.1 to 1.9
- w_query: bfloat16 [4096, 4096], P('kv', 'tp'), may hold values from -0.09375 to 0.09375
- w_forget: bfloat16 [4096, 4096], P('kv', 'tp'), may hold values from -0.09375 to 0.09375
- w_input: bfloat16 [4096, 4096], P('kv', 'tp'), may hold values from -0.09375 to 0.09375
- w_outgate: bfloat16 [4096, 4096], P('kv', 'tp'), may hold values from -0.09375 to 0.09375
- lower_bound: float32 [4096], P('tp'), may hold values from 0.3 to 0.97
- state: float32 [128, 32, 128, 128], P('kv', 'tp'), may hold values from -6 to 6
- head_gain: float32 [128], replicated, may hold values from 0.1 to 1.9
- w_mix_out: bfloat16 [4096, 4096], P('tp', 'kv'), may hold values from -0.09375 to 0.09375
- ffn_gain: float32 [4096], P('kv'), may hold values from 0.1 to 1.9
- w_gate: bfloat16 [4096, 10752], P('kv', 'tp'), may hold values from -0.09375 to 0.09375
- w_up: bfloat16 [4096, 10752], P('kv', 'tp'), may hold values from -0.09375 to 0.09375
- w_down: bfloat16 [10752, 4096], P('tp', 'kv'), may hold values from -0.0625 to 0.0625
Outputs:
- layer_out: bfloat16 [128, 4096], P(None, ('kv', 'tp'))
- new_state: float32 [128, 32, 128, 128], P('kv', 'tp')
All inputs are finite; a program needn't handle non-finite values.
Results may differ from a plain program's by a relative error of at most 0.015.
Values may be sent and summed in bfloat16 or wider, within the bound.
No kernel may reach another device: no remote copies, remote signals or barrier semaphores. Data moves between devices by JAX's collectives and lax.ppermute only.
A program may use at most 64 MiB of HBM per device.

v0:
```python
import jax
import jax.numpy as jnp
from jax import lax
from jax.sharding import PartitionSpec as P

D = 4096
DK = 128
DV = 128
EPS = 1e-06


def project_row(weight, piece):
    return jnp.dot(piece, weight, preferred_element_type=jnp.float32)


def channel_mix(rows_in, ffn_gain, w_gate, w_up, w_down):
    rows_float = rows_in.astype(jnp.float32)
    squares = jnp.sum(rows_float * rows_float, axis=1)
    scaled = (rows_float * ffn_gain).astype(jnp.bfloat16)
    gate = jnp.dot(scaled, w_gate, preferred_element_type=jnp.float32)
    upper = jnp.dot(scaled, w_up, preferred_element_type=jnp.float32)
    whole_total = lax.psum(squares, "kv")
    gate, upper = (
        lax.psum(gate.astype(jnp.bfloat16), "kv").astype(jnp.float32),
        lax.psum(upper.astype(jnp.bfloat16), "kv").astype(jnp.float32),
    )
    inverse = lax.rsqrt(whole_total / D + EPS)[:, None]
    hidden = (jax.nn.silu(gate * inverse) * (upper * inverse)).astype(jnp.bfloat16)
    terms = jnp.dot(hidden, w_down, preferred_element_type=jnp.float32)
    summed = lax.psum_scatter(
        terms.astype(jnp.bfloat16), "tp", scatter_dimension=1, tiled=True
    ).astype(jnp.float32)
    width = summed.shape[1]
    own = lax.dynamic_slice_in_dim(rows_float, lax.axis_index("tp") * width, width, 1)
    return (own + summed).astype(jnp.bfloat16)


def body(
    residual,
    mixer_gain,
    w_query,
    w_forget,
    w_input,
    w_outgate,
    lower_bound,
    state,
    head_gain,
    w_mix_out,
    ffn_gain,
    w_gate,
    w_up,
    w_down,
):
    local_seqs, local_heads = (state.shape[0], state.shape[1])
    rows = lax.all_gather(residual, "tp", axis=1, tiled=True)
    rows_float = rows.astype(jnp.float32)
    squares = jnp.sum(rows_float * rows_float, axis=1)
    scaled = (rows_float * mixer_gain).astype(jnp.bfloat16)
    part_query = jnp.dot(scaled, w_query, preferred_element_type=jnp.float32)
    part_forget = jnp.dot(scaled, w_forget, preferred_element_type=jnp.float32)
    part_value = jnp.dot(scaled, w_input, preferred_element_type=jnp.float32)
    part_gate = jnp.dot(scaled, w_outgate, preferred_element_type=jnp.float32)
    whole_total = lax.psum(squares, "kv")
    total = lax.dynamic_slice_in_dim(whole_total, lax.axis_index("kv") * local_seqs, local_seqs)
    part_query, part_forget, part_value, part_gate = (
        lax.psum_scatter(part_query, "kv", scatter_dimension=0, tiled=True),
        lax.psum_scatter(part_forget, "kv", scatter_dimension=0, tiled=True),
        lax.psum_scatter(part_value, "kv", scatter_dimension=0, tiled=True),
        lax.psum_scatter(part_gate, "kv", scatter_dimension=0, tiled=True),
    )
    inverse = lax.rsqrt(total / D + EPS)[:, None]
    bound = lower_bound.reshape(local_heads, DK)
    forget_raw = (part_forget * inverse).reshape(local_seqs, local_heads, DK)
    forget = bound + (1.0 - bound) * jax.nn.sigmoid(forget_raw)
    keyvec = (1.0 - bound) * jax.nn.sigmoid(-forget_raw)
    query = jax.nn.silu((part_query * inverse).reshape(local_seqs, local_heads, DK))
    values = (part_value * inverse).reshape(local_seqs, local_heads, DV)
    updated = forget[..., None] * state + keyvec[..., None] * values[:, :, None, :]
    head_out = jnp.einsum("shc,shce->she", query, updated, precision=lax.Precision.HIGHEST)
    inv_head = lax.rsqrt(jnp.mean(head_out * head_out, axis=2, keepdims=True) + EPS)
    out_gate = jax.nn.silu((part_gate * inverse).reshape(local_seqs, local_heads, DV))
    normed = (
        (head_out * inv_head * head_gain * out_gate)
        .reshape(local_seqs, local_heads * DV)
        .astype(jnp.bfloat16)
    )
    terms = project_row(w_mix_out, lax.all_gather(normed, "kv", axis=0, tiled=True))
    mixed = lax.psum(terms, "tp")
    after_mix = (rows_float + mixed).astype(jnp.bfloat16)
    layer_out = channel_mix(after_mix, ffn_gain, w_gate, w_up, w_down)
    return (layer_out, updated)


def solution(mesh):
    in_specs = (
        P(None, ("kv", "tp")),
        P("kv"),
        P("kv", "tp"),
        P("kv", "tp"),
        P("kv", "tp"),
        P("kv", "tp"),
        P("tp"),
        P("kv", "tp", None, None),
        P(),
        P("tp", "kv"),
        P("kv"),
        P("kv", "tp"),
        P("kv", "tp"),
        P("tp", "kv"),
    )
    out_specs = (P(None, ("kv", "tp")), P("kv", "tp", None, None))
    return jax.shard_map(body, mesh=mesh, in_specs=in_specs, out_specs=out_specs, check_vma=False)
```

profile of v0, /device:TPU:0, one launch (start us, length us, event | category | flops | bytes accessed | tf_op | source)
XLA Modules:
  0.0 312.9 jit_solution(12020792351462122957)
XLA Ops:
  7.2 15.1 %all_gather.6 = bf16[128,1024]{1,0:T(8,128)(2,1)S(1)} all-gather(bf16[128,128]{1,0:T(8,128)(2,1)} %param.14), channel_id=1, replica_groups=mesh['kv'=4,'tp'=8] {'tp'}, dimensions={1}, use_global_device_ids=true | all-gather | bytes 294912 | tf_op jit(solution)/shard_map/all_gather | solution.py:55
  22.4 2.3 fusion.10
  24.7 2.2 fusion.8
  27.0 2.3 fusion.6
  29.4 2.3 fusion.12
  31.8 9.9 %psum.35 = f32[128]{0:T(128)S(1)} all-reduce(f32[128]{0:T(128)S(1)} %fusion.1), channel_id=1, replica_groups=mesh['kv'=4,'tp'=8] {'kv'}, use_global_device_ids=true, to_apply=%region_2.0 | all-reduce | flops 128 | bytes 1024 | tf_op jit(solution)/shard_map/psum | solution.py:63
  42.5 6.5 %reduce-scatter.10.cloned.1.call-done = f32[32,512]{1,0:T(8,128)} async-done(((f32[128,512]{1,0:T(8,128)}), f32[32,512]{1,0:T(8,128)}) %reduce-scatter.10.cloned.1.call-update) | async-done | bytes 65552 | tf_op jit(solution)/shard_map/reduce_scatter | solution.py:67
  49.0 27.1 %reduce-scatter.12.cloned.1.call-done = f32[32,512]{1,0:T(8,128)} async-done(((f32[128,512]{1,0:T(8,128)}), f32[32,512]{1,0:T(8,128)}) %reduce-scatter.12.cloned.1.call-update) | async-done | bytes 65552 | tf_op jit(solution)/shard_map/reduce_scatter | solution.py:68
  76.1 27.2 %reduce-scatter.14.cloned.1.call-done = f32[32,512]{1,0:T(8,128)} async-done(((f32[128,512]{1,0:T(8,128)}), f32[32,512]{1,0:T(8,128)}) %reduce-scatter.14.cloned.1.call-update) | async-done | bytes 65552 | tf_op jit(solution)/shard_map/reduce_scatter | solution.py:69
  103.3 27.0 %reduce-scatter.8.cloned.1.call-done = f32[32,512]{1,0:T(8,128)} async-done(((f32[128,512]{1,0:T(8,128)}), f32[32,512]{1,0:T(8,128)}) %reduce-scatter.8.cloned.1.call-update) | async-done | bytes 65552 | tf_op jit(solution)/shard_map/reduce_scatter | solution.py:66
  130.3 1.0 add_divide_fusion.1
  131.6 8.2 %multiply_add_fusion = f32[32,4,128,128]{3,2,1,0:T(8,128)S(1)} fusion(f32[32,4,128,128]{3,2,1,0:T(8,128)} %param.21, f32[32,4,128]{2,1,0:T(4,128)S(1)} %mul.164, f32[32,4,128]{2,1,0:T(4,128)S(1)} %bitcast.35, f32[32,4,128]{2,1,0:T(4,128)S(1)} %bitcast.34), kind=kLoop, calls=%fused_computation | loop fusion | flops 6291456 | bytes 16973824 | tf_op jit(solution)/shard_map/add | solution.py:78
  139.9 3.4 %copy-done.1 = f32[32,4,128,128]{3,2,1,0:T(8,128)} copy-done((f32[32,4,128,128]{3,2,1,0:T(8,128)}, f32[32,4,128,128]{3,2,1,0:T(8,128)S(1)}, u32[]{:S(2)}) %copy-start.1) | copy-done | bytes 8388632
  143.2 7.2 %fusion.18 = f32[32,4,1,128]{3,2,1,0:T(1,128)S(1)} fusion(f32[32,4,128,1]{2,3,1,0:T(1,128)S(1)} %bitcast.33, f32[32,4,128,128]{3,2,1,0:T(8,128)S(1)} %multiply_add_fusion), kind=kOutput, calls=%fused_computation.39 | convolution fusion | flops 25165824 | bytes 8519680 | tf_op jit(solution)/shard_map/shc,shce->she/dot_general | solution.py:79
  150.8 8.5 %all_gather.7 = bf16[128,512]{1,0:T(8,128)(2,1)S(1)} all-gather(bf16[32,512]{1,0:T(8,128)(2,1)S(1)} %bitcast.38), channel_id=1, replica_groups=mesh['kv'=4,'tp'=8] {'kv'}, dimensions={0}, use_global_device_ids=true | all-gather | bytes 163840 | tf_op jit(solution)/shard_map/all_gather | solution.py:87
  159.2 1.1 fusion.19
  160.4 56.7 %all-reduce.4.cloned.1.call-done = f32[128,1024]{1,0:T(8,128)} async-done(((f32[128,1024]{1,0:T(8,128)}), f32[128,1024]{1,0:T(8,128)}) %all-reduce.4.cloned.1.call-update) | async-done | bytes 524304 | tf_op jit(solution)/shard_map/psum | solution.py:88
  217.1 1.2 multiply_reduce_fusion
  218.3 1.6 convolution_convert_fusion
  219.9 3.4 %convolution_convert_fusion.1 = bf16[128,1344]{0,1:T(8,128)(2,1)} fusion(bf16[1024,1344]{0,1:T(8,128)(2,1)} %param.25, f32[128,1024]{1,0:T(8,128)S(1)} %get-tuple-element.5, f32[1024]{0:T(1024)S(1)} %copy-done.3), kind=kOutput, calls=%fused_computation.2 | convolution fusion | flops 352755712 | bytes 3624960 | tf_op jit(solution)/shard_map/dot_general | solution.py:20
  223.4 10.2 %psum.38 = f32[128]{0:T(128)S(1)} all-reduce(f32[128]{0:T(128)S(1)} %get-tuple-element.4), channel_id=1, replica_groups=mesh['kv'=4,'tp'=8] {'kv'}, use_global_device_ids=true, to_apply=%region_10.11 | all-reduce | flops 128 | bytes 1024 | tf_op jit(solution)/shard_map/psum | solution.py:22
  233.6 36.4 %all-reduce.6.cloned.1.call-done = (bf16[128,1344]{0,1:T(8,128)(2,1)}, bf16[128,1344]{0,1:T(8,128)(2,1)}) async-done(((bf16[128,1344]{0,1:T(8,128)(2,1)}, bf16[128,1344]{0,1:T(8,128)(2,1)}), (bf16[128,1344]{0,1:T(8,128)(2,1)}, bf16[128,1344]{0,1:T(8,128)(2,1)})) %all-reduce.6.cloned.1.call-update) | async-done | bytes 688144 | tf_op jit(solution)/shard_map/psum | solution.py:25
  270.0 2.8 convolution_convert_fusion.2
  273.6 31.0 %reduce-scatter.16.cloned.1.call-done = bf16[128,128]{1,0:T(8,128)(2,1)} async-done(((bf16[1024,128]{1,0:T(8,128)(2,1)}), bf16[128,128]{1,0:T(8,128)(2,1)}) %reduce-scatter.16.cloned.1.call-update) | async-done | bytes 32784
  (45 shorter events, 4.1 us)
Async XLA Ops:
  7.2 211.1 %copy-start = (bf16[1024,1344]{0,1:T(8,128)(2,1)S(1)}, bf16[1024,1344]{0,1:T(8,128)(2,1)}, u32[]{:S(2)}) copy-start(bf16[1024,1344]{0,1:T(8,128)(2,1)} %param.26) | copy-start | bytes 8257540
  7.2 124.4 %copy-start.4 = (f32[512]{0:T(512)S(1)}, f32[512]{0:T(512)}, u32[]{:S(2)}) copy-start(f32[512]{0:T(512)} %param.20) | copy-start | bytes 6148
  7.2 41.8 %reduce-scatter.10.cloned.1.call-start = ((), (), s32[]{:S(2)}) async-start(), calls=%async_computation.6 | async-start | bytes 327680 | tf_op jit(solution)/shard_map/reduce_scatter | solution.py:67
  24.7 51.5 %reduce-scatter.12.cloned.1.call-start = ((), (), s32[]{:S(2)}) async-start(), calls=%async_computation.7 | async-start | bytes 327680 | tf_op jit(solution)/shard_map/reduce_scatter | solution.py:68
  27.0 76.3 %reduce-scatter.14.cloned.1.call-start = ((), (), s32[]{:S(2)}) async-start(), calls=%async_computation.8 | async-start | bytes 327680 | tf_op jit(solution)/shard_map/reduce_scatter | solution.py:69
  29.3 101.0 %reduce-scatter.8.cloned.1.call-start = ((), (), s32[]{:S(2)}) async-start(), calls=%async_computation.5 | async-start | bytes 327680 | tf_op jit(solution)/shard_map/reduce_scatter | solution.py:66
  31.7 185.4 %all-reduce.4.cloned.1.call-start = ((), (), s32[]{:S(2)}) async-start(), calls=%async_computation.9 | async-start | bytes 1048576 | tf_op jit(solution)/shard_map/psum | solution.py:88
  139.8 3.4 %copy-start.1 = (f32[32,4,128,128]{3,2,1,0:T(8,128)}, f32[32,4,128,128]{3,2,1,0:T(8,128)S(1)}, u32[]{:S(2)}) copy-start(f32[32,4,128,128]{3,2,1,0:T(8,128)S(1)} %multiply_add_fusion) | copy-start | bytes 25165828
  139.8 10.8 %copy-start.5 = (f32[128]{0:T(128)S(1)}, f32[128]{0:T(128)}, u32[]{:S(2)}) copy-start(f32[128]{0:T(128)} %param.22) | copy-start | bytes 1540
  139.9 19.4 %copy-start.2 = (bf16[512,1024]{1,0:T(8,128)(2,1)S(1)}, bf16[512,1024]{1,0:T(8,128)(2,1)}, u32[]{:S(2)}) copy-start(bf16[512,1024]{1,0:T(8,128)(2,1)} %param.23) | copy-start | bytes 3145732
  139.9 78.4 %copy-start.3 = (f32[1024]{0:T(1024)S(1)}, f32[1024]{0:T(1024)}, u32[]{:S(2)}) copy-start(f32[1024]{0:T(1024)} %param.24) | copy-start | bytes 12292
  160.4 109.6 %all-reduce.6.cloned.1.call-start = ((), (), s32[]{:S(2)}) async-start(), calls=%async_computation.11 | async-start | bytes 1376256 | tf_op jit(solution)/shard_map/psum | solution.py:25
  223.4 81.2 %reduce-scatter.16.cloned.1.call-start = ((), (), s32[]{:S(2)}) async-start(), calls=%async_computation.10 | async-start | bytes 294912
Sparse Core Ops, SparseCore 0:
  24.8 24.1 reduce-scatter.9
  51.7 24.3 reduce-scatter.11
  78.9 24.3 reduce-scatter.13
  105.9 24.3 reduce-scatter.7
  160.5 56.5 all-reduce.3
  223.5 46.4 all-reduce.5
  273.7 30.7 reduce-scatter.15
where the time goes:
time: 314 us; the launch traced here: 313 us
  waiting for transfers between devices  212 us (68%)
  blocking collectives  43.7 us (14%)
  matrix products  25.2 us (8%)
  between operations  14.3 us (5%)
  other arithmetic  12.3 us (4%)
  local copies, waits for them, and re-layouts  5.22 us (2%)
    psum x1, waiting for transfers between devices, body(): mixed = lax.psum(terms, 'tp')  56.7 us
    psum x1, waiting for transfers between devices, channel_mix(): lax.psum(upper.astype(jnp.bfloat16), 'kv').astype(jnp.float32)  36.4 us
    unnamed x8, waiting for transfers between devices  31.1 us
    reduce_scatter x1, waiting for transfers between devices, body(): lax.psum_scatter(part_gate, 'kv', scatter_dimension=0, tiled=True)  27.2 us
    reduce_scatter x1, waiting for transfers between devices, body(): lax.psum_scatter(part_value, 'kv', scatter_dimension=0, tiled=True)  27.1 us
    reduce_scatter x1, waiting for transfers between devices, body(): lax.psum_scatter(part_query, 'kv', scatter_dimension=0, tiled=True)  27 us
    all_gather x1, blocking collectives, body(): rows = lax.all_gather(residual, 'tp', axis=1, tiled=True)  15.1 us
    psum x1, blocking collectives, channel_mix(): whole_total = lax.psum(squares, 'kv')  10.2 us
  transfers between devices with their start and end apart: 7, of which 7 were waited for; matrix products, arithmetic and copies ran while one was open for 2% of the time, Pallas kernels for 0%

commit v1 on v0

--- a/solution.py
+++ b/solution.py
@@ -22,7 +22,7 @@
     whole_total = lax.psum(squares, "kv")
     gate, upper = (
         lax.psum(gate.astype(jnp.bfloat16), "kv").astype(jnp.float32),
-        lax.psum(upper.astype(jnp.bfloat16), "kv").astype(jnp.float32),
+        jnp.sum(lax.all_gather(upper.astype(jnp.bfloat16), "kv"), axis=0).astype(jnp.float32),
     )
     inverse = lax.rsqrt(whole_total / D + EPS)[:, None]
     hidden = (jax.nn.silu(gate * inverse) * (upper * inverse)).astype(jnp.bfloat16)

time: 314 us -> 335 us (1.067)
  waiting for transfers between devices: 212 us -> 225 us
  other arithmetic: 12.3 us -> 20.6 us
    all_gather x0 -> x1, waiting for transfers between devices: none -> 14.4 us  [channel_mix(): lax.all_gather(upper.astype(jnp.bfloat16), 'kv')]
    reduce_sum x0 -> x1, other arithmetic: none -> 8.94 us  [channel_mix(): jnp.sum(lax.all_gather(upper.astype(jnp.bfloat16), 'kv'), axis=0)]
    all_gather x0 -> x1, local copies, waits for them, and re-layouts: none -> 3.66 us  [channel_mix(): lax.all_gather(upper.astype(jnp.bfloat16), 'kv')]
    unnamed x8 -> x9, waiting for transfers between devices: 31.1 us -> 31.2 us
  transfers between devices with their start and end apart: 7 -> 8, of which waited for: 7 -> 8; matrix products, arithmetic and copies ran while one was open for 2% -> 7% of each run, Pallas kernels for 0% -> 0%
where the time goes in v1:
time: 335 us
  waiting for transfers between devices  225 us (67%)
  blocking collectives  43.9 us (13%)
  matrix products  25.2 us (8%)
  other arithmetic  20.6 us (6%)
  between operations  14.4 us (4%)
  local copies, waits for them, and re-layouts  5.53 us (2%)
    psum x1, waiting for transfers between devices, body(): mixed = lax.psum(terms, 'tp')  56.6 us
    psum x1, waiting for transfers between devices, channel_mix(): lax.psum(gate.astype(jnp.bfloat16), 'kv').astype(jnp.float32)  34.2 us
    unnamed x9, waiting for transfers between devices  31.2 us
    reduce_scatter x1, waiting for transfers between devices, body(): lax.psum_scatter(part_gate, 'kv', scatter_dimension=0, tiled=True)  27.1 us
    reduce_scatter x1, waiting for transfers between devices, body(): lax.psum_scatter(part_value, 'kv', scatter_dimension=0, tiled=True)  27.1 us
    reduce_scatter x1, waiting for transfers between devices, body(): lax.psum_scatter(part_query, 'kv', scatter_dimension=0, tiled=True)  27 us
    all_gather x1, blocking collectives, body(): rows = lax.all_gather(residual, 'tp', axis=1, tiled=True)  15.1 us
    all_gather x1, waiting for transfers between devices, channel_mix(): lax.all_gather(upper.astype(jnp.bfloat16), 'kv')  14.4 us
  transfers between devices with their start and end apart: 8, of which 8 were waited for; matrix products, arithmetic and copies ran while one was open for 7% of the time, Pallas kernels for 0%

profile of v1, /device:TPU:0, one launch (start us, length us, event | category | flops | bytes accessed | tf_op | source)
XLA Modules:
  0.0 334.5 jit_solution(1589188580385244822)
XLA Ops:
  7.2 15.1 %all_gather.12 = bf16[128,1024]{1,0:T(8,128)(2,1)S(1)} all-gather(bf16[128,128]{1,0:T(8,128)(2,1)} %param.14), channel_id=1, replica_groups=mesh['kv'=4,'tp'=8] {'tp'}, dimensions={1}, use_global_device_ids=true | all-gather | bytes 294912 | tf_op jit(solution)/shard_map/all_gather | solution.py:55
  22.4 2.3 fusion.10
  24.7 2.2 fusion.8
  27.1 2.2 fusion.6
  29.4 2.2 fusion.12
  31.8 9.9 %psum.28 = f32[128]{0:T(128)S(1)} all-reduce(f32[128]{0:T(128)S(1)} %fusion.1), channel_id=1, replica_groups=mesh['kv'=4,'tp'=8] {'kv'}, use_global_device_ids=true, to_apply=%region_2.0 | all-reduce | flops 128 | bytes 1024 | tf_op jit(solution)/shard_map/psum | solution.py:63
  41.8 7.1 %reduce-scatter.10.cloned.1.call-done = f32[32,512]{1,0:T(8,128)} async-done(((f32[128,512]{1,0:T(8,128)}), f32[32,512]{1,0:T(8,128)}) %reduce-scatter.10.cloned.1.call-update) | async-done | bytes 65552 | tf_op jit(solution)/shard_map/reduce_scatter | solution.py:67
  49.0 27.1 %reduce-scatter.12.cloned.1.call-done = f32[32,512]{1,0:T(8,128)} async-done(((f32[128,512]{1,0:T(8,128)}), f32[32,512]{1,0:T(8,128)}) %reduce-scatter.12.cloned.1.call-update) | async-done | bytes 65552 | tf_op jit(solution)/shard_map/reduce_scatter | solution.py:68
  76.1 27.1 %reduce-scatter.14.cloned.1.call-done = f32[32,512]{1,0:T(8,128)} async-done(((f32[128,512]{1,0:T(8,128)}), f32[32,512]{1,0:T(8,128)}) %reduce-scatter.14.cloned.1.call-update) | async-done | bytes 65552 | tf_op jit(solution)/shard_map/reduce_scatter | solution.py:69
  103.2 27.0 %reduce-scatter.8.cloned.1.call-done = f32[32,512]{1,0:T(8,128)} async-done(((f32[128,512]{1,0:T(8,128)}), f32[32,512]{1,0:T(8,128)}) %reduce-scatter.8.cloned.1.call-update) | async-done | bytes 65552 | tf_op jit(solution)/shard_map/reduce_scatter | solution.py:66
  131.5 8.2 %multiply_add_fusion = f32[32,4,128,128]{3,2,1,0:T(8,128)S(1)} fusion(f32[32,4,128,128]{3,2,1,0:T(8,128)} %param.21, f32[32,4,128]{2,1,0:T(4,128)S(1)} %mul.164, f32[32,4,128]{2,1,0:T(4,128)S(1)} %bitcast.37, f32[32,4,128]{2,1,0:T(4,128)S(1)} %bitcast.36), kind=kLoop, calls=%fused_computation | loop fusion | flops 6291456 | bytes 16973824 | tf_op jit(solution)/shard_map/add | solution.py:78
  139.8 7.2 %fusion.18 = f32[32,4,1,128]{3,2,1,0:T(1,128)S(1)} fusion(f32[32,4,128,1]{2,3,1,0:T(1,128)S(1)} %bitcast.35, f32[32,4,128,128]{3,2,1,0:T(8,128)S(1)} %multiply_add_fusion), kind=kOutput, calls=%fused_computation.39 | convolution fusion | flops 25165824 | bytes 8519680 | tf_op jit(solution)/shard_map/shc,shce->she/dot_general | solution.py:79
  147.3 8.5 %all_gather.13 = bf16[128,512]{1,0:T(8,128)(2,1)S(1)} all-gather(bf16[32,512]{1,0:T(8,128)(2,1)S(1)} %bitcast.40), channel_id=1, replica_groups=mesh['kv'=4,'tp'=8] {'kv'}, dimensions={0}, use_global_device_ids=true | all-gather | bytes 163840 | tf_op jit(solution)/shard_map/all_gather | solution.py:87
  157.0 56.6 %all-reduce.3.cloned.1.call-done = f32[128,1024]{1,0:T(8,128)} async-done(((f32[128,1024]{1,0:T(8,128)}), f32[128,1024]{1,0:T(8,128)}) %all-reduce.3.cloned.1.call-update) | async-done | bytes 524304 | tf_op jit(solution)/shard_map/psum | solution.py:88
  213.6 1.2 multiply_reduce_fusion
  214.8 1.6 convolution_convert_fusion
  216.5 3.4 %convolution_convert_fusion.1 = bf16[128,1344]{0,1:T(8,128)(2,1)} fusion(bf16[1024,1344]{0,1:T(8,128)(2,1)} %param.25, f32[128,1024]{1,0:T(8,128)S(1)} %get-tuple-element.3, f32[1024]{0:T(1024)S(1)} %copy-done.4), kind=kOutput, calls=%fused_computation.2 | convolution fusion | flops 352755712 | bytes 3624960 | tf_op jit(solution)/shard_map/dot_general | solution.py:20
  220.0 10.3 %psum.31 = f32[128]{0:T(128)S(1)} all-reduce(f32[128]{0:T(128)S(1)} %get-tuple-element.2), channel_id=1, replica_groups=mesh['kv'=4,'tp'=8] {'kv'}, use_global_device_ids=true, to_apply=%region_10.11 | all-reduce | flops 128 | bytes 1024 | tf_op jit(solution)/shard_map/psum | solution.py:22
  230.3 14.4 %all-gather.3.cloned.1.call-done = bf16[512,1344]{0,1:T(8,128)(2,1)} async-done(((bf16[128,1344]{0,1:T(8,128)(2,1)}), bf16[512,1344]{0,1:T(8,128)(2,1)}) %all-gather.3.cloned.1.call-update) | async-done | bytes 1376272 | tf_op jit(solution)/shard_map/all_gather | solution.py:25
  244.7 3.7 %reshape.65 = bf16[4,128,1344]{1,0,2:T(4,128)(2,1)} reshape(bf16[512,1344]{0,1:T(8,128)(2,1)} %all-gather.3.cloned.1.call-done) | data formatting | bytes 2752512 | tf_op jit(solution)/shard_map/all_gather | solution.py:25
  248.4 8.9 %reduce_sum.42 = bf16[128,1344]{0,1:T(8,128)(2,1)} reduce(bf16[4,128,1344]{1,0,2:T(4,128)(2,1)} %reshape.65, bf16[]{:T(256)} %constant.39.clone.1), dimensions={0}, to_apply=%region_11.12 | reduce | flops 516096 | bytes 1720322 | tf_op jit(solution)/shard_map/reduce_sum | solution.py:25
  257.3 34.2 %all-reduce.5.cloned.1.call-done = bf16[128,1344]{0,1:T(8,128)(2,1)} async-done(((bf16[128,1344]{0,1:T(8,128)(2,1)}), bf16[128,1344]{0,1:T(8,128)(2,1)}) %all-reduce.5.cloned.1.call-update) | async-done | bytes 344080 | tf_op jit(solution)/shard_map/psum | solution.py:24
  291.5 2.8 convolution_convert_fusion.2
  295.1 31.1 %reduce-scatter.16.cloned.1.call-done = bf16[128,128]{1,0:T(8,128)(2,1)} async-done(((bf16[1024,128]{1,0:T(8,128)(2,1)}), bf16[128,128]{1,0:T(8,128)(2,1)}) %reduce-scatter.16.cloned.1.call-update) | async-done | bytes 32784
  (52 shorter events, 5.7 us)
Async XLA Ops:
  7.2 207.6 %copy-start = (bf16[1024,1344]{0,1:T(8,128)(2,1)S(1)}, bf16[1024,1344]{0,1:T(8,128)(2,1)}, u32[]{:S(2)}) copy-start(bf16[1024,1344]{0,1:T(8,128)(2,1)} %param.26) | copy-start | bytes 8257540
  7.2 19.9 %copy-start.3 = (f32[1024]{0:T(1024)S(1)}, f32[1024]{0:T(1024)}, u32[]{:S(2)}) copy-start(f32[1024]{0:T(1024)} %param.15) | copy-start | bytes 12292
  7.2 41.8 %reduce-scatter.10.cloned.1.call-start = ((), (), s32[]{:S(2)}) async-start(), calls=%async_computation.6 | async-start | bytes 327680 | tf_op jit(solution)/shard_map/reduce_scatter | solution.py:67
  24.7 17.2 %copy-start.5 = (f32[512]{0:T(512)S(1)}, f32[512]{0:T(512)}, u32[]{:S(2)}) copy-start(f32[512]{0:T(512)} %param.20) | copy-start | bytes 6148
  24.7 51.4 %reduce-scatter.12.cloned.1.call-start = ((), (), s32[]{:S(2)}) async-start(), calls=%async_computation.7 | async-start | bytes 327680 | tf_op jit(solution)/shard_map/reduce_scatter | solution.py:68
  27.0 76.2 %reduce-scatter.14.cloned.1.call-start = ((), (), s32[]{:S(2)}) async-start(), calls=%async_computation.8 | async-start | bytes 327680 | tf_op jit(solution)/shard_map/reduce_scatter | solution.py:69
  29.3 100.9 %reduce-scatter.8.cloned.1.call-start = ((), (), s32[]{:S(2)}) async-start(), calls=%async_computation.5 | async-start | bytes 327680 | tf_op jit(solution)/shard_map/reduce_scatter | solution.py:66
  31.6 181.9 %all-reduce.3.cloned.1.call-start = ((), (), s32[]{:S(2)}) async-start(), calls=%async_computation.9 | async-start | bytes 1048576 | tf_op jit(solution)/shard_map/psum | solution.py:88
  139.7 7.3 %copy-start.1 = (f32[32,4,128,128]{3,2,1,0:T(8,128)}, f32[32,4,128,128]{3,2,1,0:T(8,128)S(1)}, u32[]{:S(2)}) copy-start(f32[32,4,128,128]{3,2,1,0:T(8,128)S(1)} %multiply_add_fusion) | copy-start | bytes 25165828
  139.7 7.4 %copy-start.6 = (f32[128]{0:T(128)S(1)}, f32[128]{0:T(128)}, u32[]{:S(2)}) copy-start(f32[128]{0:T(128)} %param.22) | copy-start | bytes 1540
  139.8 16.0 %copy-start.2 = (bf16[512,1024]{1,0:T(8,128)(2,1)S(1)}, bf16[512,1024]{1,0:T(8,128)(2,1)}, u32[]{:S(2)}) copy-start(bf16[512,1024]{1,0:T(8,128)(2,1)} %param.23) | copy-start | bytes 3145732
  147.0 67.7 %copy-start.4 = (f32[1024]{0:T(1024)S(1)}, f32[1024]{0:T(1024)}, u32[]{:S(2)}) copy-start(f32[1024]{0:T(1024)} %param.24) | copy-start | bytes 12292
  157.0 87.8 %all-gather.3.cloned.1.call-start = ((), (), s32[]{:S(2)}) async-start(), calls=%async_computation.11 | async-start | bytes 1720320 | tf_op jit(solution)/shard_map/all_gather | solution.py:25
  216.4 75.0 %all-reduce.5.cloned.1.call-start = ((), (), s32[]{:S(2)}) async-start(), calls=%async_computation.10 | async-start | bytes 688128 | tf_op jit(solution)/shard_map/psum | solution.py:24
  219.9 106.2 %reduce-scatter.16.cloned.1.call-start = ((), (), s32[]{:S(2)}) async-start(), calls=%async_computation.12 | async-start | bytes 294912
Sparse Core Ops, SparseCore 0:
  24.8 24.1 reduce-scatter.9
  51.7 24.3 reduce-scatter.11
  78.9 24.3 reduce-scatter.13
  105.8 24.3 reduce-scatter.7
  157.1 56.4 all-reduce.2
  216.6 28.1 all-gather.2
  247.7 43.7 all-reduce.4
  295.2 30.9 reduce-scatter.15
